TPU v7x, 32 devices: a whole 2x2x4 slice. The times are simulated.
32 devices in a mesh: gr: 2 (over x), fs: 8 (over z, y), tp: 2 (over core).
Axes of the slice: x: 2, y: 2, z: 4, core: 2. Of those that a mesh axis runs over, the one named last changes fastest.
Arguments:
- prompt: bfloat16 [3072, 2048], P(('gr', 'fs', 'tp')), may hold values from -6 to 6
- norm_first: float32 [2048], P(('gr', 'fs')), may hold values from 0.1 to 1.9
- gate_first: float32 [2048, 5632], P(('gr', 'fs'), 'tp'), may hold values from -6 to 6
- up_first: float32 [2048, 5632], P(('gr', 'fs'), 'tp'), may hold values from -6 to 6
- down_first: float32 [2048, 5632], P(('gr', 'fs'), 'tp'), may hold values from -6 to 6
- norm_second: float32 [2048], P(('gr', 'fs')), may hold values from 0.1 to 1.9
- gate_second: float32 [2048, 5632], P(('gr', 'fs'), 'tp'), may hold values from -6 to 6
- up_second: float32 [2048, 5632], P(('gr', 'fs'), 'tp'), may hold values from -6 to 6
- down_second: float32 [2048, 5632], P(('gr', 'fs'), 'tp'), may hold values from -6 to 6
Outputs:
- served_gate_first: bfloat16 [2048, 5632], P(None, 'fs')
- served_up_first: bfloat16 [2048, 5632], P(None, 'fs')
- served_down_first: bfloat16 [2048, 5632], P(None, 'fs')
- served_gate_second: bfloat16 [2048, 5632], P(None, 'fs')
- served_up_second: bfloat16 [2048, 5632], P(None, 'fs')
- served_down_second: bfloat16 [2048, 5632], P(None, 'fs')
- result: bfloat16 [3072, 2048], P(('gr', 'fs', 'tp'))
All inputs are finite; a program needn't handle non-finite values.
Results may differ from a plain program's by a relative error of at most 0.015.
Values may be sent and summed in bfloat16 or wider, within the bound.
A program may use at most 128 MiB of HBM per device.

v0:
```python
import jax
import jax.numpy as jnp
from jax import lax
from jax.sharding import PartitionSpec as P

D = 2048
FF = 5632


EPS = 1e-06


def fold_rows(gain, weight):
    return (gain[:, None] * weight).astype(jnp.bfloat16)


def relayout(stacked):
    moved = lax.all_to_all(
        lax.all_to_all(stacked, "tp", split_axis=1, concat_axis=2, tiled=True),
        "fs",
        split_axis=2,
        concat_axis=1,
        tiled=True,
    )
    whole = lax.all_gather(moved, ("gr", "tp"), axis=1, tiled=True)
    matrices = stacked.shape[0]
    block_width = moved.shape[2]
    gr_size = lax.axis_size("gr")
    tp_size = lax.axis_size("tp")
    fs_size = lax.axis_size("fs")
    sub_rows = stacked.shape[1] // tp_size
    shaped = whole.reshape(matrices, gr_size, tp_size, fs_size, sub_rows, block_width)
    return shaped.transpose(0, 1, 3, 2, 4, 5).reshape(
        matrices, gr_size * fs_size * tp_size * sub_rows, block_width
    )


def half_step(residual, weights):
    gate_weight = weights[0]
    up_weight = weights[1]
    down_weight = weights[2]
    resid_f = residual.astype(jnp.float32)
    normed = (
        resid_f * lax.rsqrt(jnp.mean(resid_f * resid_f, axis=-1, keepdims=True) + EPS)
    ).astype(jnp.bfloat16)
    in_scale = D ** (-0.5)
    out_scale = FF ** (-0.5)
    tokens_in = lax.all_gather(normed, "fs", axis=0, tiled=True)
    gate_pre = jnp.dot(tokens_in, gate_weight, preferred_element_type=jnp.float32) * in_scale
    up_pre = jnp.dot(tokens_in, up_weight, preferred_element_type=jnp.float32) * in_scale
    hidden = (jax.nn.silu(gate_pre) * up_pre).astype(jnp.bfloat16)
    branch = lax.psum_scatter(
        (
            lax.dot_general(
                hidden, down_weight, (((1,), (1,)), ((), ())), preferred_element_type=jnp.float32
            )
            * out_scale
        ).astype(jnp.bfloat16),
        "fs",
        scatter_dimension=0,
        tiled=True,
    ).astype(jnp.float32)
    return (resid_f + 0.5 * branch).astype(jnp.bfloat16)


def on_device(
    prompt,
    norm_first,
    gate_first,
    up_first,
    down_first,
    norm_second,
    gate_second,
    up_second,
    down_second,
):
    first_set = jnp.stack(
        [
            fold_rows(norm_first, gate_first),
            fold_rows(norm_first, up_first),
            down_first.astype(jnp.bfloat16),
        ]
    )
    second_set = jnp.stack(
        [
            fold_rows(norm_second, gate_second),
            fold_rows(norm_second, up_second),
            down_second.astype(jnp.bfloat16),
        ]
    )
    served_first = relayout(first_set)
    middle = half_step(prompt, served_first)
    served_second = relayout(second_set)
    result = half_step(middle, served_second)
    return (
        served_first[0],
        served_first[1],
        served_first[2],
        served_second[0],
        served_second[1],
        served_second[2],
        result,
    )


def solution(mesh):
    in_specs = (
        P(("gr", "fs", "tp"), None),
        P(("gr", "fs")),
        P(("gr", "fs"), "tp"),
        P(("gr", "fs"), "tp"),
        P(("gr", "fs"), "tp"),
        P(("gr", "fs")),
        P(("gr", "fs"), "tp"),
        P(("gr", "fs"), "tp"),
        P(("gr", "fs"), "tp"),
    )
    out_specs = (
        P(None, "fs"),
        P(None, "fs"),
        P(None, "fs"),
        P(None, "fs"),
        P(None, "fs"),
        P(None, "fs"),
        P(("gr", "fs", "tp"), None),
    )
    return jax.shard_map(
        on_device, mesh=mesh, in_specs=in_specs, out_specs=out_specs, check_vma=False
    )
```

profile of v0, /device:TPU:0, one launch (start us, length us, event | category | flops | bytes accessed | tf_op | source)
XLA Modules:
  0.0 607.6 jit_solution(7273351563624397723)
XLA Ops:
  7.2 2.5 fusion.6
  9.7 0.2 pad_maximum_fusion
  10.0 1.9 copy.52
  11.8 6.0 all_to_all.72
  17.9 2.6 copy.77
  20.5 10.8 %copy.72 = bf16[3,64,2,2816]{1,0,3,2:T(4,128)(2,1)} copy(bf16[3,64,2,2816]{3,2,1,0:T(2,128)(2,1)S(1)} %bitcast.78) | data formatting | bytes 4325376 | tf_op jit(solution)/shard_map/all_to_all | solution.py:19
  31.3 7.1 %reshape.54 = bf16[8,2,67584]{2,1,0:T(2,128)(2,1)S(1)} reshape(bf16[5632,3,64]{2,1,0:T(4,128)(2,1)} %bitcast.56) | data formatting | bytes 4325376
  38.4 57.7 %all_to_all.73 = bf16[8,2,67584]{2,1,0:T(2,128)(2,1)} all-to-all(bf16[8,2,67584]{2,1,0:T(2,128)(2,1)S(1)} %reshape.54), channel_id=1, replica_groups=mesh['gr'=2,'fs'=8,'tp'=2] {'fs'}, dimensions={0} | all-to-all | bytes 4325376 | tf_op jit(solution)/shard_map/all_to_all | solution.py:18
  96.1 8.0 %reshape.55 = bf16[5632,3,64]{2,1,0:T(4,128)(2,1)} reshape(bf16[8,2,67584]{2,1,0:T(2,128)(2,1)} %all_to_all.73) | data formatting | bytes 4325376
  104.1 9.4 %copy.55 = bf16[3,64,8,704]{3,1,2,0:T(8,128)(2,1)} copy(bf16[3,64,8,704]{1,0,3,2:T(4,128)(2,1)} %bitcast.57) | data formatting | bytes 4325376 | tf_op jit(solution)/shard_map/all_to_all | solution.py:18
  113.8 0.9 fusion.1
  114.7 0.3 reduce-scatter.3.cloned.1.call-start
  115.0 61.3 %all-gather.5.cloned.1.call-done = bf16[3,2048,704]{2,1,0:T(8,128)(2,1)} async-done(((bf16[3,512,704]{2,1,0:T(8,128)(2,1)}), bf16[3,2048,704]{2,1,0:T(8,128)(2,1)}) %all-gather.5.cloned.1.call-update) | async-done | bytes 8650768 | tf_op jit(solution)/shard_map/all_gather | solution.py:25
  176.3 4.1 fusion.15
  180.4 0.3 copy.56
  180.8 1.9 copy.57
  182.6 1.8 copy.58
  184.5 54.6 %all-gather.9.cloned.1.call-done = bf16[768,2048]{1,0:T(8,128)(2,1)} async-done(((bf16[96,2048]{1,0:T(8,128)(2,1)}), bf16[768,2048]{1,0:T(8,128)(2,1)}) %all-gather.9.cloned.1.call-update) | async-done | bytes 3145744 | tf_op jit(solution)/shard_map/all_gather | solution.py:48
  239.1 5.7 fusion.16
  244.8 12.4 %multiply_convert_fusion.1 = bf16[768,2048]{1,0:T(8,128)(2,1)} fusion(bf16[2048,704]{1,0:T(8,128)(2,1)} %bitcast.64, f32[768,704]{0,1:T(8,128)} %fusion.16, bf16[768,2048]{1,0:T(8,128)(2,1)} %all-gather.9.cloned.1.call-done, bf16[2048,704]{1,0:T(8,128)(2,1)} %bitcast.62), kind=kOutput, calls=%fused_computation.1 | convolution fusion | flops 4436656128 | bytes 14221312 | tf_op jit(solution)/shard_map/dot_general | solution.py:54
  257.3 0.5 all-gather.7.cloned.1.call-start
  257.9 2.5 fusion.8
  260.6 1.9 copy.59
  262.5 6.0 all_to_all.74
  268.5 3.9 copy.76
  272.5 15.1 %copy.73 = bf16[3,64,2,2816]{1,0,3,2:T(4,128)(2,1)} copy(bf16[3,64,2,2816]{3,2,1,0:T(2,128)(2,1)} %bitcast.79) | data formatting | bytes 4325376 | tf_op jit(solution)/shard_map/all_to_all | solution.py:19
  287.6 8.2 %reshape.56 = bf16[8,2,67584]{2,1,0:T(2,128)(2,1)} reshape(bf16[5632,3,64]{2,1,0:T(4,128)(2,1)} %bitcast.58) | data formatting | bytes 4325376
  295.9 67.8 %all_to_all.75 = bf16[8,2,67584]{2,1,0:T(2,128)(2,1)} all-to-all(bf16[8,2,67584]{2,1,0:T(2,128)(2,1)} %reshape.56), channel_id=1, replica_groups=mesh['gr'=2,'fs'=8,'tp'=2] {'fs'}, dimensions={0} | all-to-all | bytes 4325376 | tf_op jit(solution)/shard_map/all_to_all | solution.py:18
  363.7 8.0 %reshape.57 = bf16[5632,3,64]{2,1,0:T(4,128)(2,1)} reshape(bf16[8,2,67584]{2,1,0:T(2,128)(2,1)} %all_to_all.75) | data formatting | bytes 4325376
  371.6 9.4 %copy.62 = bf16[3,64,8,704]{3,1,2,0:T(8,128)(2,1)} copy(bf16[3,64,8,704]{1,0,3,2:T(4,128)(2,1)} %bitcast.59) | data formatting | bytes 4325376 | tf_op jit(solution)/shard_map/all_to_all | solution.py:18
  381.1 1.3 fusion.3
  382.4 1.9 fusion.4
  384.5 59.3 %all-gather.7.cloned.1.call-done = bf16[3,2048,704]{2,1,0:T(8,128)(2,1)} async-done(((bf16[3,512,704]{2,1,0:T(8,128)(2,1)}), bf16[3,2048,704]{2,1,0:T(8,128)(2,1)}) %all-gather.7.cloned.1.call-update) | async-done | bytes 8650768 | tf_op jit(solution)/shard_map/all_gather | solution.py:25
  443.8 4.1 fusion.14
  447.9 1.9 copy.63
  449.8 1.9 copy.64
  451.7 1.9 copy.65
  453.6 52.8 %all-gather.11.cloned.1.call-done = bf16[768,2048]{1,0:T(8,128)(2,1)} async-done(((bf16[96,2048]{1,0:T(8,128)(2,1)}), bf16[768,2048]{1,0:T(8,128)(2,1)}) %all-gather.11.cloned.1.call-update) | async-done | bytes 3145744 | tf_op jit(solution)/shard_map/all_gather | solution.py:48
  506.5 6.6 %fusion.17 = f32[768,704]{0,1:T(8,128)} fusion(bf16[768,2048]{1,0:T(8,128)(2,1)} %all-gather.11.cloned.1.call-done, bf16[2048,704]{1,0:T(8,128)(2,1)} %bitcast.66), kind=kOutput, calls=%fused_computation.39 | convolution fusion | flops 2214592512 | bytes 8192000 | tf_op jit(solution)/shard_map/dot_general | solution.py:49
  513.1 12.4 %multiply_convert_fusion = bf16[768,2048]{1,0:T(8,128)(2,1)} fusion(bf16[2048,704]{1,0:T(8,128)(2,1)} %bitcast.70, f32[768,704]{0,1:T(8,128)} %fusion.17, bf16[768,2048]{1,0:T(8,128)(2,1)} %all-gather.11.cloned.1.call-done, bf16[2048,704]{1,0:T(8,128)(2,1)} %bitcast.68), kind=kOutput, calls=%fused_computation | convolution fusion | flops 4436656128 | bytes 14221312 | tf_op jit(solution)/shard_map/dot_general | solution.py:54
  525.6 4.6 copy.69
  530.1 4.6 copy.70
  534.7 4.6 copy.71
  539.2 2.7 copy.66
  541.9 4.7 copy.67
  546.7 2.7 copy.68
  549.3 49.1 %reduce-scatter.5.cloned.1.call-done = bf16[96,2048]{1,0:T(8,128)(2,1)} async-done(((bf16[768,2048]{1,0:T(8,128)(2,1)}), bf16[96,2048]{1,0:T(8,128)(2,1)}) %reduce-scatter.5.cloned.1.call-update) | async-done | bytes 393232 | tf_op jit(solution)/shard_map/reduce_scatter | solution.py:52
  598.5 2.1 fusion.5
  (21 shorter events, 1.0 us)
Async XLA Ops:
  7.2 169.1 %all-gather.5.cloned.1.call-start = ((), (), s32[]{:S(2)}) async-start(), calls=%async_computation.6 | async-start | bytes 11796480 | tf_op jit(solution)/shard_map/all_gather | solution.py:25
  104.1 9.5 %copy-start.1 = (bf16[96,2048]{1,0:T(8,128)(2,1)S(1)}, bf16[96,2048]{1,0:T(8,128)(2,1)}, u32[]{:S(2)}) copy-start(bf16[96,2048]{1,0:T(8,128)(2,1)} %param.9) | copy-start | bytes 1179652
  113.5 125.6 %all-gather.9.cloned.1.call-start = ((), (), s32[]{:S(2)}) async-start(), calls=%async_computation.8 | async-start | bytes 3538944 | tf_op jit(solution)/shard_map/all_gather | solution.py:48
  114.7 266.4 %reduce-scatter.3.cloned.1.call-start = ((), (), s32[]{:S(2)}) async-start(), calls=%async_computation.9 | async-start | bytes 3538944 | tf_op jit(solution)/shard_map/reduce_scatter | solution.py:52
  257.2 0.7 copy-start.2
  257.3 186.5 %all-gather.7.cloned.1.call-start = ((), (), s32[]{:S(2)}) async-start(), calls=%async_computation.7 | async-start | bytes 11796480 | tf_op jit(solution)/shard_map/all_gather | solution.py:25
  381.0 125.4 %all-gather.11.cloned.1.call-start = ((), (), s32[]{:S(2)}) async-start(), calls=%async_computation.10 | async-start | bytes 3538944 | tf_op jit(solution)/shard_map/all_gather | solution.py:48
  384.3 214.2 %reduce-scatter.5.cloned.1.call-start = ((), (), s32[]{:S(2)}) async-start(), calls=%async_computation.11 | async-start | bytes 3538944 | tf_op jit(solution)/shard_map/reduce_scatter | solution.py:52
  541.9 4.7 copy-start
Sparse Core Ops, SparseCore 0:
  113.6 62.6 all-gather.4
  179.1 60.0 all-gather.8
  257.4 96.6 reduce-scatter.2
  381.2 62.5 all-gather.6
  446.4 60.0 all-gather.10
  525.7 72.7 reduce-scatter.4
where the time goes:
time: 615 us; the launch traced here: 608 us
  waiting for transfers between devices  277 us (45%)
  blocking collectives  138 us (22%)
  local copies, waits for them, and re-layouts  128 us (21%)
  matrix products  37.2 us (6%)
  between operations  14.4 us (2%)
  other arithmetic  11.8 us (2%)
    all_to_all x2, blocking collectives, relayout(): lax.all_to_all(lax.all_to_all(stacked, 'tp', split_axis=1, concat_axis=2,...  126 us
    all_gather x2, waiting for transfers between devices, relayout(): whole = lax.all_gather(moved, ('gr', 'tp'), axis=1, tiled=True)  121 us
    all_gather x2, waiting for transfers between devices, half_step(): tokens_in = lax.all_gather(normed, 'fs', axis=0, tiled=True)  107 us
    unnamed x16, local copies, waits for them, and re-layouts  55.2 us
    reduce_scatter x2, waiting for transfers between devices, half_step(): lax.psum_scatter((lax.dot_general(hidden, down_weight, (((1,), (1,)), (()...  49.1 us
    all_to_all x4, local copies, waits for them, and re-layouts, relayout(): lax.all_to_all(stacked, 'tp', split_axis=1, concat_axis=2, tiled=True)  32.4 us
    dot_general x2, matrix products, half_step(): lax.dot_general(hidden, down_weight, (((1,), (1,)), ((), ())), preferred_...  24.9 us
    all_to_all x2, local copies, waits for them, and re-layouts, relayout(): lax.all_to_all(lax.all_to_all(stacked, 'tp', split_axis=1, concat_axis=2,...  18.8 us
  transfers between devices with their start and end apart: 6, of which 5 were waited for; matrix products, arithmetic and copies ran while one was open for 16% of the time, Pallas kernels for 0%

commit v1 on v0

v1 whole, which is shorter than its diff:
```python
import functools

import jax
import jax.numpy as jnp
from jax import lax
from jax.experimental import pallas as pl
from jax.experimental.pallas import tpu as pltpu
from jax.sharding import PartitionSpec as P

EPS = 1e-06
MESH = pl.DeviceIdType.MESH


def fold_rows(gain, weight):
    return (gain[:, None] * weight).astype(jnp.bfloat16)


def relayout_kernel(sizes, pieces, *refs):
    gr, fs, tp = sizes
    mats, blocks, rows, _ = pieces.shape
    outs = refs[:mats]
    first_send, first_recv, gr_send, gr_recv, tp_send, tp_recv = refs[mats:]
    g, f, t = lax.axis_index("gr"), lax.axis_index("fs"), lax.axis_index("tp")
    sub = rows // tp

    def rows_of(m, from_gr, from_fs, core):
        start = pl.multiple_of((from_gr * fs + from_fs) * rows + core * sub, sub)
        return outs[m].at[pl.ds(start, sub)]

    def remote(src, dst, send_sem, recv_sem, device):
        return pltpu.make_async_remote_copy(
            src_ref=src,
            dst_ref=dst,
            send_sem=send_sem,
            recv_sem=recv_sem,
            device_id=device,
            device_id_type=MESH,
        )

    def first_copies(step, act):
        slot = (step + f) % blocks
        block = t * blocks + slot
        for core in range(tp):
            mine = jnp.logical_and(block == f, t == core)
            for m in range(mats):
                source = pieces.at[m, slot, pl.ds(core * sub, sub)]
                target = rows_of(m, g, f, core)
                act(
                    mine,
                    lambda: pltpu.make_async_copy(source, target, first_recv.at[m, f]),
                    lambda: remote(
                        source,
                        target,
                        first_send.at[m, slot, core],
                        first_recv.at[m, f],
                        (g, block, core),
                    ),
                )

    def start(mine, local, far):
        @pl.when(mine)
        def _():
            local().start()

        @pl.when(jnp.logical_not(mine))
        def _():
            far().start()

    def finish(mine, local, far):
        @pl.when(jnp.logical_not(mine))
        def _():
            far().wait_send()

    def origin(step):
        return ((f // blocks + step % tp) % tp) * blocks + (f + blocks - step // tp) % blocks

    def to_peers(m, ref):
        for hop in range(1, tp):
            remote(ref, ref, tp_send.at[m], tp_recv.at[m], (g, f, (t + hop) % tp)).start()

    def send_first(step, carry):
        first_copies(step, start)
        return carry

    def pass_on(step, carry):
        source = origin(step)
        for m in range(mats):
            ref = rows_of(m, g, source, t)
            pltpu.make_async_copy(ref, ref, first_recv.at[m, source]).wait()
            for hop in range(1, gr):
                remote(
                    ref,
                    ref,
                    gr_send.at[m],
                    gr_recv.at[m, hop - 1, source],
                    ((g + hop) % gr, f, t),
                ).start()
            to_peers(m, ref)
        return carry

    def pass_on_far(step, carry):
        source = origin(step)
        for m in range(mats):
            for hop in range(1, gr):
                ref = rows_of(m, (g + gr - hop) % gr, source, t)
                pltpu.make_async_copy(ref, ref, gr_recv.at[m, hop - 1, source]).wait()
                to_peers(m, ref)
        return carry

    def finish_first(step, carry):
        first_copies(step, finish)
        return carry

    lax.fori_loop(0, blocks, send_first, 0)
    lax.fori_loop(0, fs, pass_on, 0)
    lax.fori_loop(0, fs, pass_on_far, 0)
    lax.fori_loop(0, blocks, finish_first, 0)

    def wait_rows(m, count, sem):
        if count:
            ref = outs[m].at[pl.ds(0, count)]
            pltpu.make_async_copy(ref, ref, sem).wait()

    for m in range(mats):
        wait_rows(m, fs * sub * (gr - 1), gr_send.at[m])
        wait_rows(m, gr * fs * sub * (tp - 1), tp_send.at[m])
        wait_rows(m, gr * fs * sub * (tp - 1), tp_recv.at[m])


def relayout(pieces, sizes):
    gr, fs, tp = sizes
    mats, blocks, rows, width = pieces.shape
    total = gr * fs * rows
    served = jax.ShapeDtypeStruct((total, width), pieces.dtype)
    return pl.pallas_call(
        functools.partial(relayout_kernel, sizes),
        out_shape=[served] * mats,
        in_specs=[pl.BlockSpec(memory_space=pltpu.VMEM)],
        out_specs=[pl.BlockSpec(memory_space=pl.ANY)] * mats,
        scratch_shapes=[
            pltpu.SemaphoreType.DMA((mats, blocks, tp)),
            pltpu.SemaphoreType.DMA((mats, fs)),
            pltpu.SemaphoreType.DMA((mats,)),
            pltpu.SemaphoreType.DMA((mats, max(gr - 1, 1), fs)),
            pltpu.SemaphoreType.DMA((mats,)),
            pltpu.SemaphoreType.DMA((mats,)),
        ],
        compiler_params=pltpu.CompilerParams(has_side_effects=True),
        cost_estimate=pl.CostEstimate(
            flops=0, bytes_accessed=mats * total * width * 24, transcendentals=0
        ),
        name="relayout",
    )(pieces)


def cut(matrices, blocks):
    rows, columns = matrices[0].shape
    return jnp.stack(
        [m.reshape(rows, blocks, columns // blocks).transpose(1, 0, 2) for m in matrices]
    )


def normed_tokens(resid_f):
    return (
        resid_f * lax.rsqrt(jnp.mean(resid_f * resid_f, axis=-1, keepdims=True) + EPS)
    ).astype(jnp.bfloat16)


def partial_branch(tokens_in, weights):
    gate_weight, up_weight, down_weight = weights
    in_scale = gate_weight.shape[0] ** (-0.5)
    out_scale = (down_weight.shape[1] * lax.axis_size("fs")) ** (-0.5)
    gate_pre = jnp.dot(tokens_in, gate_weight, preferred_element_type=jnp.float32) * in_scale
    up_pre = jnp.dot(tokens_in, up_weight, preferred_element_type=jnp.float32) * in_scale
    hidden = (jax.nn.silu(gate_pre) * up_pre).astype(jnp.bfloat16)
    return (
        lax.dot_general(
            hidden, down_weight, (((1,), (1,)), ((), ())), preferred_element_type=jnp.float32
        )
        * out_scale
    ).astype(jnp.bfloat16)


def gather_tokens(normed):
    return lax.all_gather(normed, "fs", axis=0, tiled=True)


def scatter_sum(partial):
    return lax.psum_scatter(partial, "fs", scatter_dimension=0, tiled=True)


def on_device(
    prompt,
    norm_first,
    gate_first,
    up_first,
    down_first,
    norm_second,
    gate_second,
    up_second,
    down_second,
):
    sizes = tuple(lax.axis_size(axis) for axis in ("gr", "fs", "tp"))
    blocks = sizes[1] // sizes[2]
    prompt_f = prompt.astype(jnp.float32)
    tokens_first = gather_tokens(normed_tokens(prompt_f))
    pieces_first = cut(
        [
            fold_rows(norm_first, gate_first),
            fold_rows(norm_first, up_first),
            down_first.astype(jnp.bfloat16),
        ],
        blocks,
    )
    pieces_second = cut(
        [
            fold_rows(norm_second, gate_second),
            fold_rows(norm_second, up_second),
            down_second.astype(jnp.bfloat16),
        ],
        blocks,
    )
    served_first = relayout(pieces_first, sizes)
    partial_first = partial_branch(tokens_first, served_first)
    pieces_second, partial_first = lax.optimization_barrier((pieces_second, partial_first))
    served_second = relayout(pieces_second, sizes)
    branch_first = scatter_sum(partial_first).astype(jnp.float32)
    middle = (prompt_f + 0.5 * branch_first).astype(jnp.bfloat16)
    middle_f = middle.astype(jnp.float32)
    tokens_second = gather_tokens(normed_tokens(middle_f))
    branch_second = scatter_sum(partial_branch(tokens_second, served_second)).astype(jnp.float32)
    result = (middle_f + 0.5 * branch_second).astype(jnp.bfloat16)
    return (*served_first, *served_second, result)


def solution(mesh):
    in_specs = (
        P(("gr", "fs", "tp"), None),
        P(("gr", "fs")),
        P(("gr", "fs"), "tp"),
        P(("gr", "fs"), "tp"),
        P(("gr", "fs"), "tp"),
        P(("gr", "fs")),
        P(("gr", "fs"), "tp"),
        P(("gr", "fs"), "tp"),
        P(("gr", "fs"), "tp"),
    )
    out_specs = (
        P(None, "fs"),
        P(None, "fs"),
        P(None, "fs"),
        P(None, "fs"),
        P(None, "fs"),
        P(None, "fs"),
        P(("gr", "fs", "tp"), None),
    )
    return jax.shard_map(
        on_device, mesh=mesh, in_specs=in_specs, out_specs=out_specs, check_vma=False
    )
```

time: 615 us -> 435 us (0.71); the launches traced: 608 us -> 434 us
  Pallas kernels: 0 us -> 201 us
  waiting for transfers between devices: 277 us -> 127 us
  blocking collectives: 138 us -> 0 us
  local copies, waits for them, and re-layouts: 128 us -> 41 us
    all_gather x4 -> x2, waiting for transfers between devices: 228 us -> 0.02 us  [gather_tokens(): return lax.all_gather(normed, 'fs', axis=0, tiled=True)]
    pallas_call x0 -> x2, Pallas kernels: none -> 201 us  [relayout(): pl.pallas_call(functools.partial(relayout_kernel, sizes), out_shape=[serv...]
    all_to_all x4 -> x0, blocking collectives: 138 us -> none  [the longest x2 126 us: relayout(): lax.all_to_all(lax.all_to_all(stacked, 'tp', split_axis=1, concat_axis=2,...]
    reduce_scatter x2, waiting for transfers between devices: 49.1 us -> 127 us  [scatter_sum(): return lax.psum_scatter(partial, 'fs', scatter_dimension=0, tiled=True)]
    all_to_all x6 -> x0, local copies, waits for them, and re-layouts: 51.2 us -> none  [the longest x4 32.4 us: relayout(): lax.all_to_all(stacked, 'tp', split_axis=1, concat_axis=2, tiled=True)]
    unnamed x16 -> x48, local copies, waits for them, and re-layouts: 55.2 us -> 30.2 us
    slice x8 -> x0, local copies, waits for them, and re-layouts: 17.9 us -> none  [the longest x2 5.99 us: on_device(): served_second[2]]
    reshape x0 -> x6, local copies, waits for them, and re-layouts: none -> 10.8 us  [cut(): m.reshape(rows, blocks, columns // blocks).transpose(1, 0, 2)]
  transfers between devices with their start and end apart: 6 -> 4, of which waited for: 5 -> 2; matrix products, arithmetic and copies ran while one was open for 16% -> 10% of each run, Pallas kernels for 0% -> 46%
where the time goes in v1:
time: 435 us; the launch traced here: 434 us
  Pallas kernels  201 us (46%)
  waiting for transfers between devices  127 us (29%)
  local copies, waits for them, and re-layouts  41 us (9%)
  matrix products  36.7 us (8%)
  other arithmetic  14.3 us (3%)
  between operations  13.9 us (3%)
    pallas_call x2, Pallas kernels, relayout(): pl.pallas_call(functools.partial(relayout_kernel, sizes), out_shape=[serv...  201 us
    reduce_scatter x2, waiting for transfers between devices, scatter_sum(): return lax.psum_scatter(partial, 'fs', scatter_dimension=0, tiled=True)  127 us
    unnamed x48, local copies, waits for them, and re-layouts  30.2 us
    dot_general x2, matrix products, partial_branch(): lax.dot_general(hidden, down_weight, (((1,), (1,)), ((), ())), preferred_...  23.1 us
    dot_general x2, matrix products, partial_branch(): jnp.dot(tokens_in, gate_weight, preferred_element_type=jnp.float32)  13.6 us
    reshape x6, local copies, waits for them, and re-layouts, cut(): m.reshape(rows, blocks, columns // blocks).transpose(1, 0, 2)  10.8 us
  transfers between devices with their start and end apart: 4, of which 2 were waited for; matrix products, arithmetic and copies ran while one was open for 10% of the time, Pallas kernels for 46%

profile of v1, /device:TPU:0, one launch (start us, length us, event | category | flops | bytes accessed | tf_op | source)
XLA Modules:
  0.0 433.9 jit_solution(14707132692169517699)
XLA Ops:
  7.2 0.0 all-gather.3.cloned.1.call-start
  7.2 1.3 fusion
  8.5 1.9 fusion.1
  10.4 0.0 all-gather.3.cloned.1.call-update
  10.4 0.0 reduce-scatter.3.cloned.1.call-start
  10.5 0.3 copy.26
  10.8 0.0 copy-start.13
  10.8 1.2 copy.27
  12.0 0.5 copy-done.13
  12.5 0.3 copy.32
  12.8 1.2 copy.33
  14.0 0.5 copy-done.14
  14.5 0.4 copy.22
  14.9 1.8 copy.24
  16.7 1.3 multiply_convert_fusion.7
  18.1 2.4 copy.25
  20.4 2.3 copy.23
  22.7 0.4 copy.28
  23.2 1.8 copy.30
  25.0 1.3 multiply_convert_fusion.5
  26.3 1.5 copy.31
  27.8 2.3 copy.29
  30.1 1.7 pad_maximum_fusion.pieces
  31.8 96.1 %relayout.2 = (bf16[2048,704]{1,0:T(8,128)(2,1)}, bf16[2048,704]{1,0:T(8,128)(2,1)}, bf16[2048,704]{1,0:T(8,128)(2,1)}) custom-call(bf16[3,4,128,704]{3,2,1,0:T(8,128)(2,1)} %pad_maximum_fusion.pieces), custom_call_target="tpu_custom_call" | custom-call | bytes 103809024 | tf_op jit(solution)/shard_map/relayout/pallas_call | solution.py:135
  128.0 1.7 pad_maximum_fusion.1.pieces
  129.7 6.8 %fusion.10 = f32[768,704]{0,1:T(8,128)} fusion(bf16[768,2048]{1,0:T(8,128)(2,1)} %all-gather.3.cloned.1.call-done, bf16[2048,704]{1,0:T(8,128)(2,1)} %get-tuple-element.30), kind=kOutput, calls=%fused_computation.28 | convolution fusion | flops 2214592512 | bytes 8192000 | tf_op jit(solution)/shard_map/dot_general | solution.py:173
  136.5 11.5 %multiply_convert_fusion.1 = bf16[768,2048]{1,0:T(8,128)(2,1)} fusion(bf16[2048,704]{1,0:T(8,128)(2,1)S(1)} %copy-done.8, f32[768,704]{0,1:T(8,128)} %fusion.10, bf16[768,2048]{1,0:T(8,128)(2,1)} %all-gather.3.cloned.1.call-done, bf16[2048,704]{1,0:T(8,128)(2,1)} %get-tuple-element.31), kind=kOutput, calls=%fused_computation.1 | convolution fusion | flops 4436656128 | bytes 14221312 | tf_op jit(solution)/shard_map/dot_general | solution.py:177
  148.0 0.0 reduce-scatter.3.cloned.1.call-update
  148.0 0.0 all-gather.5.cloned.1.call-start
  148.1 77.1 %reduce-scatter.3.cloned.1.call-done = bf16[96,2048]{1,0:T(8,128)(2,1)} async-done(((bf16[768,2048]{1,0:T(8,128)(2,1)}), bf16[96,2048]{1,0:T(8,128)(2,1)}) %reduce-scatter.3.cloned.1.call-update) | async-done | bytes 393232 | tf_op jit(solution)/shard_map/reduce_scatter | solution.py:189
  225.1 1.2 fusion.3
  226.4 1.9 fusion.4
  228.3 0.0 all-gather.5.cloned.1.call-update
  228.3 0.0 reduce-scatter.5.cloned.1.call-start
  228.4 105.1 %relayout.3 = (bf16[2048,704]{1,0:T(8,128)(2,1)}, bf16[2048,704]{1,0:T(8,128)(2,1)}, bf16[2048,704]{1,0:T(8,128)(2,1)}) custom-call(bf16[3,4,128,704]{3,2,1,0:T(8,128)(2,1)} %pad_maximum_fusion.1.pieces), custom_call_target="tpu_custom_call" | custom-call | bytes 103809024 | tf_op jit(solution)/shard_map/relayout/pallas_call | solution.py:135
  333.5 0.0 all-gather.5.cloned.1.call-done
  333.5 6.8 %fusion.11 = f32[768,704]{0,1:T(8,128)} fusion(bf16[768,2048]{1,0:T(8,128)(2,1)} %all-gather.5.cloned.1.call-done, bf16[2048,704]{1,0:T(8,128)(2,1)} %get-tuple-element.33), kind=kOutput, calls=%fused_computation.29 | convolution fusion | flops 2214592512 | bytes 8192000 | tf_op jit(solution)/shard_map/dot_general | solution.py:173
  340.3 11.6 %multiply_convert_fusion = bf16[768,2048]{1,0:T(8,128)(2,1)} fusion(bf16[2048,704]{1,0:T(8,128)(2,1)S(1)} %copy-done.10, f32[768,704]{0,1:T(8,128)} %fusion.11, bf16[768,2048]{1,0:T(8,128)(2,1)} %all-gather.5.cloned.1.call-done, bf16[2048,704]{1,0:T(8,128)(2,1)} %get-tuple-element.34), kind=kOutput, calls=%fused_computation | convolution fusion | flops 4436656128 | bytes 14221312 | tf_op jit(solution)/shard_map/dot_general | solution.py:177
  351.9 0.0 reduce-scatter.5.cloned.1.call-update
  351.9 1.9 copy-done.9
  353.8 2.7 copy.35
  356.4 4.7 %copy.36 = bf16[2048,704]{0,1:T(8,128)(2,1)} copy(bf16[2048,704]{1,0:T(8,128)(2,1)} %get-tuple-element.32) | data formatting | bytes 5767168
  361.2 2.7 copy.34
  363.9 4.7 %copy.38 = bf16[2048,704]{0,1:T(8,128)(2,1)} copy(bf16[2048,704]{1,0:T(8,128)(2,1)} %get-tuple-element.34) | data formatting | bytes 5767168
  368.6 2.7 copy.39
  371.3 4.6 %copy.37 = bf16[2048,704]{0,1:T(8,128)(2,1)} copy(bf16[2048,704]{1,0:T(8,128)(2,1)} %get-tuple-element.33) | data formatting | bytes 5767168
  375.9 49.5 %reduce-scatter.5.cloned.1.call-done = bf16[96,2048]{1,0:T(8,128)(2,1)} async-done(((bf16[768,2048]{1,0:T(8,128)(2,1)}), bf16[96,2048]{1,0:T(8,128)(2,1)}) %reduce-scatter.5.cloned.1.call-update) | async-done | bytes 393232 | tf_op jit(solution)/shard_map/reduce_scatter | solution.py:189
  425.4 1.9 fusion.5
  (35 shorter events, 0.1 us)
Async XLA Ops:
  7.2 3.3 copy-start.12
  7.2 122.5 %all-gather.3.cloned.1.call-start = ((), (), s32[]{:S(2)}) async-start(), calls=%async_computation.2 | async-start | bytes 3538944 | tf_op jit(solution)/shard_map/all_gather | solution.py:185
  10.4 214.7 %reduce-scatter.3.cloned.1.call-start = ((), (), s32[]{:S(2)}) async-start(), calls=%async_computation.3 | async-start | bytes 3538944 | tf_op jit(solution)/shard_map/reduce_scatter | solution.py:189
  10.8 1.7 copy-start.13
  12.8 1.7 copy-start.14
  14.5 2.2 copy-start.16
  18.1 4.7 %copy-start.15 = (f32[128,2816]{1,0:T(8,128)S(1)}, f32[128,2816]{1,0:T(8,128)}, u32[]{:S(2)}) copy-start(f32[128,2816]{1,0:T(8,128)} %param.15) | copy-start | bytes 4325380
  22.7 2.2 copy-start.17
  26.3 3.8 copy-start.3
  26.3 3.8 copy-start.4
  26.3 3.8 copy-start.5
  31.8 96.1 %copy-start.2 = (bf16[128,4,704]{2,0,1:T(8,128)(2,1)S(1)}, bf16[128,4,704]{2,0,1:T(8,128)(2,1)}, u32[]{:S(2)}) copy-start(bf16[128,4,704]{2,0,1:T(8,128)(2,1)} %copy.33) | copy-start | bytes 2162692
  31.8 96.1 %copy-start.6 = (bf16[128,4,704]{2,0,1:T(8,128)(2,1)S(1)}, bf16[128,4,704]{2,0,1:T(8,128)(2,1)}, u32[]{:S(2)}) copy-start(bf16[128,4,704]{2,0,1:T(8,128)(2,1)} %copy.29) | copy-start | bytes 2162692
  129.7 6.8 %copy-start.8 = (bf16[2048,704]{1,0:T(8,128)(2,1)S(1)}, bf16[2048,704]{1,0:T(8,128)(2,1)}, u32[]{:S(2)}) copy-start(bf16[2048,704]{1,0:T(8,128)(2,1)} %get-tuple-element.32) | copy-start | bytes 8650756
  148.0 77.2 %copy-start = (bf16[96,2048]{1,0:T(8,128)(2,1)S(1)}, bf16[96,2048]{1,0:T(8,128)(2,1)}, u32[]{:S(2)}) copy-start(bf16[96,2048]{1,0:T(8,128)(2,1)} %param.9) | copy-start | bytes 1179652
  148.0 185.5 %all-gather.5.cloned.1.call-start = ((), (), s32[]{:S(2)}) async-start(), calls=%async_computation.4 | async-start | bytes 3538944 | tf_op jit(solution)/shard_map/all_gather | solution.py:185
  228.3 197.1 %reduce-scatter.5.cloned.1.call-start = ((), (), s32[]{:S(2)}) async-start(), calls=%async_computation.5 | async-start | bytes 3538944 | tf_op jit(solution)/shard_map/reduce_scatter | solution.py:189
  333.5 6.8 %copy-start.10 = (bf16[2048,704]{1,0:T(8,128)(2,1)S(1)}, bf16[2048,704]{1,0:T(8,128)(2,1)}, u32[]{:S(2)}) copy-start(bf16[2048,704]{1,0:T(8,128)(2,1)} %get-tuple-element.35) | copy-start | bytes 8650756
  351.9 1.9 copy-start.9
  356.4 4.7 %copy-start.7 = (bf16[2048,704]{1,0:T(8,128)(2,1)S(1)}, bf16[2048,704]{1,0:T(8,128)(2,1)}, u32[]{:S(2)}) copy-start(bf16[2048,704]{1,0:T(8,128)(2,1)} %get-tuple-element.30) | copy-start | bytes 8650756
  363.9 4.7 %copy-start.11 = (bf16[2048,704]{1,0:T(8,128)(2,1)S(1)}, bf16[2048,704]{1,0:T(8,128)(2,1)}, u32[]{:S(2)}) copy-start(bf16[2048,704]{1,0:T(8,128)(2,1)} %get-tuple-element.35) | copy-start | bytes 8650756
  371.3 54.1 %copy-start.1 = (bf16[96,2048]{1,0:T(8,128)(2,1)S(1)}, bf16[96,2048]{1,0:T(8,128)(2,1)}, u32[]{:S(2)}) copy-start(bf16[96,2048]{1,0:T(8,128)(2,1)} %reduce-scatter.3.cloned.1.call-done) | copy-start | bytes 1179652
Sparse Core Ops, SparseCore 0:
  10.7 82.2 all-gather.2
  148.1 76.9 reduce-scatter.2
  228.4 90.9 all-gather.4
  352.0 73.3 reduce-scatter.4
